TPU v7x, 128 devices: a whole 4x4x4 slice. The times are simulated.
128 devices in a mesh: sp: 16 (over z, y), fs: 4 (over x), tp: 2 (over core).
Axes of the slice: x: 4, y: 4, z: 4, core: 2. Of those that a mesh axis runs over, the one named last changes fastest.
Arguments:
- tokens: bfloat16 [4, 4096, 2048], P('fs', 'sp', 'tp'), may hold values from -6 to 6
- norm_gain: float32 [2048], replicated, may hold values from 0.1 to 1.9
- lin_query: bfloat16 [2048, 1024], P(None, ('fs', 'tp')), may hold values from -0.125 to 0.125
- lin_key: bfloat16 [2048, 1024], P(None, ('fs', 'tp')), may hold values from -0.125 to 0.125
- lin_value: bfloat16 [2048, 2048], P(None, ('fs', 'tp')), may hold values from -0.125 to 0.125
- lin_decay: bfloat16 [2048, 1024], P(None, ('fs', 'tp')), may hold values from -0.125 to 0.125
- decay_bias: float32 [1024], replicated, may hold values from -0.5 to 8.5
- decay_shift: bfloat16 [2, 4, 4096], P(None, 'fs', 'sp'), may hold values from -1.4 to 1.5, as said below
- soft_query: bfloat16 [2048, 2048], P(None, ('fs', 'tp')), may hold values from -0.190034947 to 0.190034947
- soft_key: bfloat16 [2048, 2048], P(None, ('fs', 'tp')), may hold values from -1.9887378 to 1.9887378
- soft_value: bfloat16 [2048, 2048], P(None, ('fs', 'tp')), may hold values from -0.125 to 0.125
- soft_lambda: float32 [8], replicated, may hold values from 0.3 to 0.8
- lin_gain: float32 [256], replicated, may hold values from 0.1 to 1.9
- soft_gain: float32 [256], replicated, may hold values from 0.1 to 1.9
- lin_out: bfloat16 [2048, 2048], P(('fs', 'tp')), may hold values from -0.09375 to 0.09375
- soft_out: bfloat16 [2048, 2048], P(('fs', 'tp')), may hold values from -0.09375 to 0.09375
Outputs:
- mixed: bfloat16 [4, 4096, 2048], P('fs', 'sp', 'tp')
- log_mass: float32 [8, 2, 4, 4096], P(('fs', 'tp'), None, None, 'sp')
Inputs may be any that keep to these rules, and one draw needn't show every extreme that they name: `decay_shift`: row 1 is never positive.
All inputs are finite; a program needn't handle non-finite values.
Results may differ from a plain program's by a relative error of at most 0.02.
Values may be sent and summed in bfloat16 or wider, within the bound.
No kernel may reach another device: no remote copies, remote signals or barrier semaphores. Data moves between devices by JAX's collectives and lax.ppermute only.
A program may use at most 192 MiB of HBM per device.

v0:
```python
import jax
import jax.numpy as jnp
from jax import lax
from jax.sharding import Mesh
from jax.sharding import PartitionSpec as P

GLA_KEY = 128
GLA_VALUE = 256
DIFF_HEAD = 128
DIFF_VALUE = 256
BLOCK = 64
SP = ("sp_0", "sp_1")
norm_eps = 1e-06
decay_tau = 16.0
rope_base = 500000.0


def neutral_like(array, identity):
    return jax.tree.map(
        lambda a, e: jnp.broadcast_to(jnp.asarray(e, a.dtype), a.shape), array, identity
    )


def carried_in(array, axes, combine, identity):
    before = start = neutral_like(array, identity)
    running = array
    for axis in reversed(axes):
        length, place = (lax.axis_size(axis), lax.axis_index(axis))
        pieces = jax.tree.map(
            lambda part, kind: lax.all_gather(part.astype(kind), axis),
            running,
            (jnp.bfloat16, jnp.bfloat16),
        )
        inside, running = (start, start)
        for k in range(length):
            passed = k < place
            running = combine(
                running, jax.tree.map(lambda part, own: part[k].astype(own.dtype), pieces, array)
            )
            inside = jax.tree.map(lambda new, old: jnp.where(passed, new, old), running, inside)
        before = combine(inside, before)
    return before


def scaled_rms(values, norm_gain):
    return (
        values * lax.rsqrt(jnp.mean(values * values, axis=-1, keepdims=True) + norm_eps) * norm_gain
    )


def rotate(values, positions):
    half_dim = values.shape[-1] // 2
    inv_freq = jnp.power(
        jnp.float32(rope_base), -jnp.arange(half_dim, dtype=jnp.float32) * (2.0 / values.shape[-1])
    )
    angles = positions.astype(jnp.float32)[:, None] * inv_freq[None, :]
    cos_table = jnp.cos(angles)[:, None, None, :]
    sin_table = jnp.sin(angles)[:, None, None, :]
    widened = values.astype(jnp.float32)
    first_half = widened[..., :half_dim]
    second_half = widened[..., half_dim:]
    turned = jnp.concatenate(
        [
            first_half * cos_table - second_half * sin_table,
            second_half * cos_table + first_half * sin_table,
        ],
        axis=-1,
    )
    return turned.astype(jnp.bfloat16)


def block_pass(queries, key_rows, value_rows, log_decay, block_len):
    groups, length, heads, key_dim = queries.shape
    value_dim = value_rows.shape[-1]
    block_count = length // block_len

    def split(tensor):
        return tensor.reshape(groups, block_count, block_len, heads, tensor.shape[-1]).transpose(
            1, 0, 3, 2, 4
        )

    causal = jnp.tril(jnp.ones((block_len, block_len), dtype=bool))[:, :, None]

    def advance(carry, inputs):
        state_now, offset = carry
        query_blk, key_blk, value_blk, decay_blk = inputs
        cum_log = jnp.cumsum(decay_blk, axis=2)
        inner_part = jnp.einsum("bhcd,bhdv->bhcv", query_blk * jnp.exp(cum_log), state_now)
        decay_pair = jnp.exp(
            jnp.where(causal, cum_log[:, :, :, None, :] - cum_log[:, :, None, :, :], -jnp.inf)
        )
        scores = jnp.sum(
            query_blk[:, :, :, None, :] * key_blk[:, :, None, :, :] * decay_pair, axis=-1
        )
        local_part = jnp.einsum("bhij,bhjv->bhiv", scores, value_blk)
        last_log = cum_log[:, :, -1, :]
        state_now = jnp.exp(last_log)[..., None] * state_now + jnp.einsum(
            "bhcd,bhcv->bhdv", key_blk * jnp.exp(last_log[:, :, None, :] - cum_log), value_blk
        )
        carried = query_blk * jnp.exp(offset[:, :, None, :] + cum_log)
        return ((state_now, offset + last_log), (inner_part + local_part, carried))

    start = (
        jnp.zeros((groups, heads, key_dim, value_dim), jnp.float32),
        jnp.zeros((groups, heads, key_dim), jnp.float32),
    )
    (state_end, offset_end), (outs, carried) = lax.scan(
        advance, start, (split(queries), split(key_rows), split(value_rows), split(log_decay))
    )
    return (outs, carried, state_end, offset_end)


def project(rows, weight):
    lead_shape = rows.shape[:-1]
    flat_rows = rows.reshape(-1, rows.shape[-1])
    product = jnp.dot(flat_rows, weight, preferred_element_type=jnp.float32)
    return product.reshape(lead_shape + (weight.shape[1],))


def chain_join(earlier, later):
    return (earlier[0] * later[0], later[0][..., None] * earlier[1] + later[1])


def attend(queries, query_pos, reach, all_keys, all_values, soft_lambda, soft_gain, rows_dev):
    groups, query_rows, soft_heads = queries.shape[:3]
    block_total = all_keys.shape[1] // rows_dev
    scale = DIFF_HEAD ** (-0.5)

    def first_pass(block_id, carry):
        top_now, total_now, score_store = carry
        key_blk = lax.dynamic_slice_in_dim(all_keys, block_id * rows_dev, rows_dev, 1)
        raw_scores = (
            jnp.einsum("bqhmd,bkhmd->bhmqk", queries, key_blk, preferred_element_type=jnp.float32)
            * scale
        )
        key_pos = block_id * rows_dev + jnp.arange(rows_dev, dtype=jnp.int32)
        scores = jnp.where(key_pos[None, :] <= query_pos[:, None], raw_scores, -jnp.inf)
        top_next = jnp.maximum(top_now, jnp.max(scores, axis=-1))
        total_next = total_now * jnp.exp(top_now - top_next) + jnp.sum(
            jnp.exp(scores - top_next[..., None]), axis=-1
        )
        score_store = lax.dynamic_update_index_in_dim(score_store, scores, block_id, 0)
        return (top_next, total_next, score_store)

    stat_shape = (groups, soft_heads, 2, query_rows)
    store_init = jnp.full((block_total,) + stat_shape + (rows_dev,), -jnp.inf, jnp.float32)
    top_all, total_all, score_store = lax.fori_loop(
        0,
        reach,
        first_pass,
        (
            jnp.full(stat_shape, -jnp.inf, jnp.float32),
            jnp.zeros(stat_shape, jnp.float32),
            store_init,
        ),
    )
    mass = top_all + jnp.log(total_all)

    def second_pass(block_id, accum):
        scores = lax.dynamic_index_in_dim(score_store, block_id, 0, keepdims=False)
        probs = jnp.exp(scores - top_all[..., None]) / total_all[..., None]
        weights = (probs[:, :, 0] - soft_lambda[None, :, None, None] * probs[:, :, 1]).astype(
            jnp.bfloat16
        )
        value_blk = lax.dynamic_slice_in_dim(all_values, block_id * rows_dev, rows_dev, 1)
        return accum + jnp.einsum(
            "bhqk,bkhv->bhqv", weights, value_blk, preferred_element_type=jnp.float32
        )

    accum = lax.fori_loop(
        0, reach, second_pass, jnp.zeros((groups, soft_heads, query_rows, DIFF_VALUE), jnp.float32)
    )
    soft_mix = scaled_rms(accum, soft_gain).astype(jnp.bfloat16).transpose(0, 2, 1, 3)
    soft_mix = soft_mix.reshape(groups, query_rows, soft_heads * DIFF_VALUE)
    return (soft_mix, mass)


def mixers(
    normed,
    shift_rows,
    lin_query,
    lin_key,
    lin_value,
    lin_decay,
    decay_bias,
    soft_query,
    soft_key,
    soft_value,
    soft_lambda,
    lin_gain,
    soft_gain,
):
    groups, rows_dev, model_width = normed.shape
    lin_heads = lin_query.shape[1] // GLA_KEY
    soft_heads = soft_value.shape[1] // DIFF_VALUE
    place = lax.axis_index(SP)
    shift_wide = shift_rows.astype(jnp.float32)
    lin_q = (
        project(normed, lin_query)
        .astype(jnp.bfloat16)
        .reshape(groups, rows_dev, lin_heads, GLA_KEY)
    )
    lin_k = (
        project(normed, lin_key).astype(jnp.bfloat16).reshape(groups, rows_dev, lin_heads, GLA_KEY)
    )
    lin_v = (
        project(normed, lin_value)
        .astype(jnp.bfloat16)
        .reshape(groups, rows_dev, lin_heads, GLA_VALUE)
    )
    gate_input = project(normed, lin_decay) + decay_bias + shift_wide[0][:, :, None]
    log_decay = jax.nn.log_sigmoid(gate_input) / decay_tau + shift_wide[1][:, :, None]
    log_decay = log_decay.reshape(groups, rows_dev, lin_heads, GLA_KEY)
    outs, carried, state_end, offset_end = block_pass(
        lin_q.astype(jnp.float32),
        lin_k.astype(jnp.float32),
        lin_v.astype(jnp.float32),
        log_decay,
        BLOCK,
    )
    keep_in, state_in = carried_in(
        (jnp.exp(offset_end), state_end),
        SP,
        chain_join,
        (jnp.ones_like(offset_end), jnp.zeros_like(state_end)),
    )
    outs = outs + jnp.einsum("nbhcd,bhdv->nbhcv", carried, state_in)
    lin_raw = outs.transpose(1, 0, 3, 2, 4).reshape(groups, rows_dev, lin_heads, GLA_VALUE)
    lin_mix = (
        scaled_rms(lin_raw, lin_gain)
        .astype(jnp.bfloat16)
        .reshape(groups, rows_dev, lin_heads * GLA_VALUE)
    )
    positions = place * rows_dev + jnp.arange(rows_dev, dtype=jnp.int32)
    soft_q = rotate(
        project(normed, soft_query)
        .astype(jnp.bfloat16)
        .reshape(groups, rows_dev, soft_heads, 2, DIFF_HEAD),
        positions,
    )
    soft_k = rotate(
        project(normed, soft_key)
        .astype(jnp.bfloat16)
        .reshape(groups, rows_dev, soft_heads, 2, DIFF_HEAD),
        positions,
    )
    soft_v = (
        project(normed, soft_value)
        .astype(jnp.bfloat16)
        .reshape(groups, rows_dev, soft_heads, DIFF_VALUE)
    )
    all_keys, all_values = (
        lax.all_gather(soft_k, SP, axis=1, tiled=True),
        lax.all_gather(soft_v, SP, axis=1, tiled=True),
    )
    soft_mix, mass = attend(
        soft_q, positions, place + 1, all_keys, all_values, soft_lambda, soft_gain, rows_dev
    )
    return (lin_mix, soft_mix, mass)


def output_term(lin_mix, soft_mix, lin_out, soft_out, rows_dev, parts):
    col_width = lin_out.shape[1] // parts

    def term(start, row_count):
        pieces = []
        for turn_index in range(row_count // rows_dev):
            piece_id = (start + turn_index * rows_dev) // rows_dev
            seq_id = piece_id // parts
            part_id = piece_id % parts
            lin_rows = lax.dynamic_index_in_dim(lin_mix, seq_id, 0, keepdims=False)
            soft_rows = lax.dynamic_index_in_dim(soft_mix, seq_id, 0, keepdims=False)
            lin_cols = lax.dynamic_slice_in_dim(lin_out, part_id * col_width, col_width, 1)
            soft_cols = lax.dynamic_slice_in_dim(soft_out, part_id * col_width, col_width, 1)
            pieces.append(
                jnp.dot(lin_rows, lin_cols, preferred_element_type=jnp.float32)
                + jnp.dot(soft_rows, soft_cols, preferred_element_type=jnp.float32)
            )
        return jnp.concatenate(pieces, axis=0)

    return term


def shards(
    tokens,
    norm_gain,
    lin_query,
    lin_key,
    lin_value,
    lin_decay,
    decay_bias,
    decay_shift,
    soft_query,
    soft_key,
    soft_value,
    soft_lambda,
    lin_gain,
    soft_gain,
    lin_out,
    soft_out,
):
    rows_dev = tokens.shape[1]
    parts = lax.axis_size("tp")
    fs_size = lax.axis_size("fs")
    fs_index = lax.axis_index("fs")
    tp_index = lax.axis_index("tp")
    whole = lax.all_gather(tokens, "tp", axis=2, tiled=True).astype(jnp.float32)
    normed = scaled_rms(whole, norm_gain).astype(jnp.bfloat16)
    lambda_grid = soft_lambda.reshape(fs_size, parts, -1)
    bias_grid = decay_bias.reshape(fs_size, parts, -1)
    all_rows, all_shift = (
        lax.all_gather(normed, "fs", axis=0, tiled=True),
        lax.all_gather(decay_shift, "fs", axis=1, tiled=True),
    )
    head_lambda = lax.dynamic_index_in_dim(
        lax.dynamic_index_in_dim(lambda_grid, fs_index, 0, keepdims=False),
        tp_index,
        0,
        keepdims=False,
    )
    head_bias = lax.dynamic_index_in_dim(
        lax.dynamic_index_in_dim(bias_grid, fs_index, 0, keepdims=False),
        tp_index,
        0,
        keepdims=False,
    )
    lin_mix, soft_mix, mass = mixers(
        all_rows,
        all_shift,
        lin_query,
        lin_key,
        lin_value,
        lin_decay,
        head_bias,
        soft_query,
        soft_key,
        soft_value,
        head_lambda,
        lin_gain,
        soft_gain,
    )
    term = output_term(lin_mix, soft_mix, lin_out, soft_out, rows_dev, parts)
    summed = lax.psum_scatter(
        term(jnp.int32(0), rows_dev * lax.axis_size(("fs", "tp"))).astype(jnp.bfloat16),
        ("fs", "tp"),
        scatter_dimension=0,
        tiled=True,
    ).astype(jnp.float32)
    log_mass = mass.transpose(1, 2, 0, 3)
    mixed = summed.astype(jnp.bfloat16).reshape(1, rows_dev, summed.shape[1])
    return (mixed, log_mass)


def solution(mesh):
    split = Mesh(
        mesh.devices.reshape(4, 4, mesh.shape["fs"], mesh.shape["tp"]), ("sp_0", "sp_1", "fs", "tp")
    )
    placed = (
        P("fs", SP, "tp"),
        P(),
        P(None, ("fs", "tp")),
        P(None, ("fs", "tp")),
        P(None, ("fs", "tp")),
        P(None, ("fs", "tp")),
        P(),
        P(None, "fs", SP),
        P(None, ("fs", "tp")),
        P(None, ("fs", "tp")),
        P(None, ("fs", "tp")),
        P(),
        P(),
        P(),
        P(("fs", "tp"), None),
        P(("fs", "tp"), None),
    )
    return jax.shard_map(
        shards,
        mesh=split,
        in_specs=placed,
        out_specs=(P("fs", SP, "tp"), P(("fs", "tp"), None, None, SP)),
        check_vma=False,
    )
```

profile of v0, /device:TPU:0, one launch (start us, length us, event | category | flops | bytes accessed | tf_op | source)
XLA Modules:
  0.0 483.6 jit_solution(4084504965831790650)
XLA Ops:
  8.0 15.9 %all-gather.10.cloned.1.call-done = bf16[1,256,2048]{2,1,0:T(8,128)(2,1)} async-done(((bf16[1,256,1024]{2,1,0:T(8,128)(2,1)}), bf16[1,256,2048]{2,1,0:T(8,128)(2,1)}) %all-gather.10.cloned.1.call-update) | async-done | bytes 1048592 | tf_op jit(solution)/shard_map/all_gather | solution.py:307
  25.4 2.6 fusion.48
  28.1 9.8 %all_gather.37 = bf16[2,4,256]{2,0,1:T(2,128)(2,1)S(1)} all-gather(bf16[2,1,256]{2,0,1:T(2,128)(2,1)S(1)} %copy-done.14), channel_id=1, replica_groups=mesh['sp_0'=4,'sp_1'=4,'fs'=4,'tp'=2] {'fs'}, dimensions={1}, use_global_device_ids=true | all-gather | bytes 5120 | tf_op jit(solution)/shard_map/all_gather | solution.py:313
  38.6 39.1 %all-gather.12.cloned.1.call-done = bf16[4,256,2048]{2,1,0:T(8,128)(2,1)} async-done(((bf16[1,256,2048]{2,1,0:T(8,128)(2,1)}), bf16[4,256,2048]{2,1,0:T(8,128)(2,1)}) %all-gather.12.cloned.1.call-update) | async-done | bytes 4194320 | tf_op jit(solution)/shard_map/all_gather | solution.py:312
  77.7 3.8 fusion.100
  85.5 21.9 %while.44 = (s32[]{:T(128)}, f32[4,1,128,256]{3,2,0,1:T(8,128)S(1)}, f32[4,1,128]{2,0,1:T(4,128)S(1)}, f32[4,4,1,64,256]{4,3,0,1,2:T(8,128)}, bf16[4,4,1,64,128]...) while((s32[]{:T(128)}, ...), condition=%wide.region_4.5_spmd.clone, body=%wide.region_1.4_spmd.clone.sunk | while | flops 55235584 | bytes 4980881 | solution.py:107
  85.8 3.7 multiply_reduce_fusion.3
  91.3 3.7 multiply_reduce_fusion.3
  96.7 3.7 multiply_reduce_fusion.3
  102.2 3.7 multiply_reduce_fusion.3
  108.8 11.1 %all-gather = bf16[16,1,128]{2,1,0:T(2,128)(2,1)S(1)} all-gather(bf16[4,1,128]{2,1,0:T(2,128)(2,1)S(1)} %copy.118), channel_id=2, replica_groups=mesh['sp_0'=4,'sp_1'=4,'fs'=4,'tp'=2] {'sp_1'}, dimensions={0}, use_global_device_ids=true | all-gather | bytes 5120 | tf_op jit(solution)/shard_map/all_gather | solution.py:30
  120.0 12.8 %all-gather.18.cloned.1.call-done = bf16[16,1,128,256]{3,2,1,0:T(8,128)(2,1)} async-done(((bf16[4,1,128,256]{3,2,1,0:T(8,128)(2,1)}), bf16[16,1,128,256]{3,2,1,0:T(8,128)(2,1)}) %all-gather.18.cloned.1.call-update) | async-done | bytes 1048592 | tf_op jit(solution)/shard_map/all_gather | solution.py:30
  132.8 2.2 fusion.153
  135.3 3.8 convolution_convert_fusion.2
  139.9 3.8 convolution_convert_fusion.1
  146.2 2.5 copy.161
  148.6 2.8 subtract_convert_fusion
  152.6 4.7 convolution_convert_fusion
  158.2 10.1 %all_gather.40 = bf16[4,4,1,128]{3,1,2,0:T(4,128)(2,1)S(1)} all-gather(bf16[1,4,1,128]{3,1,2,0:T(4,128)(2,1)S(1)} %fusion.174), channel_id=1, replica_groups=mesh['sp_0'=4,'sp_1'=4,'fs'=4,'tp'=2] {'sp_0'}, dimensions={0}, use_global_device_ids=true | all-gather | bytes 5120 | tf_op jit(solution)/shard_map/all_gather | solution.py:30
  168.7 3.6 fusion.73
  184.2 48.9 %all-gather.16.cloned.1.call-done = bf16[4,4096,1,2,128]{4,1,3,0,2:T(8,128)(2,1)} async-done(((bf16[4,256,1,2,128]{4,1,3,0,2:T(8,128)(2,1)}), bf16[4,4096,1,2,128]{4,1,3,0,2:T(8,128)(2,1)}) %all-gather.16.cloned.1.call-update) | async-done | bytes 8388624 | tf_op jit(solution)/shard_map/all_gather | solution.py:253
  233.1 11.3 %broadcast_in_dim.60 = f32[16,4,1,2,256,256]{4,5,3,1,2,0:T(8,128)} broadcast(f32[]{:T(128)} %constant.670.clone.1), dimensions={} | broadcast | bytes 33554436 | tf_op jit(solution)/shard_map/broadcast_in_dim | solution.py:146
  244.4 3.6 while.43
  246.1 1.6 bitcast_dynamic-update-slice_fusion.2
  248.7 57.0 %all-gather.20.cloned.1.call-done = bf16[4,4096,256]{2,1,0:T(8,128)(2,1)} async-done(((bf16[4,256,256]{2,1,0:T(8,128)(2,1)}), bf16[4,4096,256]{2,1,0:T(8,128)(2,1)}) %all-gather.20.cloned.1.call-update) | async-done | bytes 8388624 | tf_op jit(solution)/shard_map/all_gather | solution.py:254
  305.8 7.7 %while.42 = (s32[]{:T(128)}, f32[4,1,256,256]{3,2,0,1:T(8,128)S(1)}, s32[]{:T(128)}, f32[16,4,1,2,256,256]{4,5,3,1,2,0:T(8,128)}, f32[4,1,2,256]{3,0,2,1:T(4,128...) while((s32[]{:T(128)}, ...), condition=%wide.region_11.12_spmd, body=%wide.region_10.11_spmd.sunk | while | flops 136314880 | bytes 17318612 | solution.py:170
  305.8 1.8 constant_dynamic-slice_fusion.3
  307.6 1.9 copy.191
  309.5 1.9 fusion.213
  311.4 2.0 fusion.214
  314.0 2.7 fusion.51
  324.5 152.2 %reduce-scatter.2.cloned.1.call-done = bf16[256,1024]{1,0:T(8,128)(2,1)} async-done(((bf16[2048,1024]{1,0:T(8,128)(2,1)}), bf16[256,1024]{1,0:T(8,128)(2,1)}) %reduce-scatter.2.cloned.1.call-update) | async-done | bytes 524304 | tf_op jit(solution)/shard_map/reduce_scatter | solution.py:343
  (174 shorter events, 43.7 us)
Async XLA Ops:
  7.2 74.3 %copy-start = (bf16[2048,256]{1,0:T(8,128)(2,1)S(1)}, bf16[2048,256]{1,0:T(8,128)(2,1)}, u32[]{:S(2)}) copy-start(bf16[2048,256]{1,0:T(8,128)(2,1)} %param.26) | copy-start | bytes 3145732
  7.2 20.9 %copy-start.14 = (bf16[2,1,256]{2,0,1:T(2,128)(2,1)S(1)}, bf16[2,1,256]{2,0,1:T(2,128)(2,1)}, u32[]{:S(2)}) copy-start(bf16[2,1,256]{2,0,1:T(2,128)(2,1)} %param.29) | copy-start | bytes 3076
  7.2 70.5 %copy-start.19 = (bf16[2048,128]{1,0:T(8,128)(2,1)S(1)}, bf16[2048,128]{1,0:T(8,128)(2,1)}, u32[]{:S(2)}) copy-start(bf16[2048,128]{1,0:T(8,128)(2,1)} %param.27) | copy-start | bytes 1572868
  7.2 16.7 %all-gather.10.cloned.1.call-start = ((), (), s32[]{:S(2)}) async-start(), calls=%async_computation.1 | async-start | bytes 1572864 | tf_op jit(solution)/shard_map/all_gather | solution.py:307
  7.9 69.7 %all-gather.12.cloned.1.call-start = ((), (), s32[]{:S(2)}) async-start(), calls=%async_computation.2 | async-start | bytes 5242880 | tf_op jit(solution)/shard_map/all_gather | solution.py:312
  28.0 104.8 %all-gather.18.cloned.1.call-start = ((), (), s32[]{:S(2)}) async-start(), calls=%async_computation.6 | async-start | bytes 1310720 | tf_op jit(solution)/shard_map/all_gather | solution.py:30
  77.7 3.8 copy-start.18
  81.5 1.3 copy-start.20
  82.8 1.3 copy-start.21
  107.4 0.8 copy-start.22
  108.2 60.5 %all-gather.14.cloned.1.call-start = ((), (), s32[]{:S(2)}) async-start(), calls=%async_computation.3 | async-start | bytes 1310720 | tf_op jit(solution)/shard_map/all_gather | solution.py:30
  135.1 98.0 %all-gather.16.cloned.1.call-start = ((), (), s32[]{:S(2)}) async-start(), calls=%async_computation.4 | async-start | bytes 8912896 | tf_op jit(solution)/shard_map/all_gather | solution.py:253
  152.5 4.9 %copy-start.17 = (f32[8]{0:T(128)S(1)}, f32[8]{0:T(128)}, u32[]{:S(2)}) copy-start(f32[8]{0:T(128)} %param.33) | copy-start | bytes 100
  152.5 15.8 %copy-start.11 = (bf16[4,256,1,2,64]{4,1,3,0,2:T(8,128)(2,1)S(1)}, bf16[4,256,1,2,64]{4,1,3,0,2:T(8,128)(2,1)}, u32[]{:S(2)}) copy-start(bf16[4,256,1,2,64]{4,1,3,0,2:T(8,128)(2,1)} %get-tuple-element.303) | copy-start | bytes 786436
  152.5 15.8 %copy-start.12 = (bf16[4,256,1,2,64]{4,1,3,0,2:T(8,128)(2,1)S(1)}, bf16[4,256,1,2,64]{4,1,3,0,2:T(8,128)(2,1)}, u32[]{:S(2)}) copy-start(bf16[4,256,1,2,64]{4,1,3,0,2:T(8,128)(2,1)} %get-tuple-element.304) | copy-start | bytes 786436
  152.6 16.1 %copy-start.13 = (bf16[16,1,128,256]{3,2,1,0:T(8,128)(2,1)S(1)}, bf16[16,1,128,256]{3,2,1,0:T(8,128)(2,1)}, u32[]{:S(2)}) copy-start(bf16[16,1,128,256]{3,2,1,0:T(8,128)(2,1)} %all-gather.18.cloned.1.call-done) | copy-start | bytes 3145732
  152.6 153.1 %all-gather.20.cloned.1.call-start = ((), (), s32[]{:S(2)}) async-start(), calls=%async_computation.7 | async-start | bytes 8912896 | tf_op jit(solution)/shard_map/all_gather | solution.py:254
  157.4 15.1 %copy-start.15 = (f32[256]{0:T(256)S(1)}, f32[256]{0:T(256)}, u32[]{:S(2)}) copy-start(f32[256]{0:T(256)} %param.34) | copy-start | bytes 3076
  157.4 319.3 %reduce-scatter.2.cloned.1.call-start = ((), (), s32[]{:S(2)}) async-start(), calls=%async_computation.5 | async-start | bytes 4718592 | tf_op jit(solution)/shard_map/reduce_scatter | solution.py:343
  168.6 5.3 %copy-start.3 = (bf16[256,2048]{1,0:T(8,128)(2,1)S(1)}, bf16[256,2048]{1,0:T(8,128)(2,1)}, u32[]{:S(2)}) copy-start(bf16[256,2048]{1,0:T(8,128)(2,1)} %param.36) | copy-start | bytes 3145732
  305.7 8.0 %copy-start.16 = (f32[256]{0:T(256)S(1)}, f32[256]{0:T(256)}, u32[]{:S(2)}) copy-start(f32[256]{0:T(256)} %param.35) | copy-start | bytes 3076
  313.5 3.2 copy-start.2
  313.5 3.2 copy-start.10
  313.5 4.3 copy-start.9
  313.7 5.2 %copy-start.8 = (f32[256,1024]{1,0:T(8,128)S(1)}, f32[256,1024]{1,0:T(8,128)}, u32[]{:S(2)}) copy-start(f32[256,1024]{1,0:T(8,128)} %fusion.127) | copy-start | bytes 3145732
  314.0 6.1 %copy-start.7 = (f32[256,1024]{1,0:T(8,128)S(1)}, f32[256,1024]{1,0:T(8,128)}, u32[]{:S(2)}) copy-start(f32[256,1024]{1,0:T(8,128)} %fusion.137) | copy-start | bytes 3145732
  316.7 4.5 copy-start.6
  317.8 4.4 copy-start.5
  318.9 4.4 copy-start.4
  321.2 155.6 %copy-start.1 = (bf16[2048,256]{1,0:T(8,128)(2,1)S(1)}, bf16[2048,256]{1,0:T(8,128)(2,1)}, u32[]{:S(2)}) copy-start(bf16[2048,256]{1,0:T(8,128)(2,1)} %param.26) | copy-start | bytes 3145732
Sparse Core Ops, SparseCore 0:
  9.7 14.1 all-gather.9
  28.1 49.5 all-gather.11
  108.3 24.4 all-gather.17
  135.2 24.6 all-gather.13
  161.9 71.1 all-gather.15
  235.1 70.5 all-gather.19
  324.6 152.0 reduce-scatter.1
where the time goes:
time: 487 us; the launch traced here: 484 us
  waiting for transfers between devices  327 us (67%)
  matrix products  53.4 us (11%)
  other arithmetic  32.7 us (7%)
  blocking collectives  31.1 us (6%)
  local copies, waits for them, and re-layouts  24.3 us (5%)
  between operations  14.7 us (3%)
    reduce_scatter x1, waiting for transfers between devices, shards(): lax.psum_scatter(term(jnp.int32(0), rows_dev * lax.axis_size(('fs', 'tp')...  152 us
    all_gather x1, waiting for transfers between devices, mixers(): lax.all_gather(soft_v, SP, axis=1, tiled=True)  57 us
    all_gather x1, waiting for transfers between devices, mixers(): lax.all_gather(soft_k, SP, axis=1, tiled=True)  48.9 us
    all_gather x1, waiting for transfers between devices, shards(): lax.all_gather(normed, 'fs', axis=0, tiled=True)  39.1 us
    all_gather x2, blocking collectives, carried_in(): lax.all_gather(part.astype(kind), axis)  21.3 us
    dot_general x7, matrix products, project(): product = jnp.dot(flat_rows, weight, preferred_element_type=jnp.float32)  19.8 us
    all_gather x1, waiting for transfers between devices, shards(): whole = lax.all_gather(tokens, 'tp', axis=2, tiled=True).astype(jnp.float32)  15.9 us
    reduce_sum x4, other arithmetic, advance(): jnp.sum(query_blk[:, :, :, None, :] * key_blk[:, :, None, :, :] * decay_p...  14.9 us
  transfers between devices with their start and end apart: 7, of which 6 were waited for; matrix products, arithmetic and copies ran while one was open for 11% of the time, Pallas kernels for 0%

commit v1 on v0

--- a/solution.py
+++ b/solution.py
@@ -250,7 +250,7 @@
         .reshape(groups, rows_dev, soft_heads, DIFF_VALUE)
     )
     all_keys, all_values = (
-        lax.all_gather(soft_k, SP, axis=1, tiled=True),
+        jnp.concatenate(lax.all_to_all(jnp.stack([soft_k] * lax.axis_size(SP)), SP, 0, 0), axis=1),
         lax.all_gather(soft_v, SP, axis=1, tiled=True),
     )
     soft_mix, mass = attend(

time: 487 us -> 565 us (1.16)
  blocking collectives: 31.1 us -> 113 us
  waiting for transfers between devices: 327 us -> 306 us
  local copies, waits for them, and re-layouts: 24.3 us -> 37.1 us
  starting transfers between devices: 0.47 us -> 6.74 us
    all_gather x2, blocking collectives: 21.3 us -> 103 us  [carried_in(): lax.all_gather(part.astype(kind), axis)]
    all_gather x1, waiting for transfers between devices: 57 us -> 0.01 us  [mixers(): lax.all_gather(soft_v, SP, axis=1, tiled=True)]
    all_gather x1 -> x0, waiting for transfers between devices: 48.9 us -> none  [mixers(): lax.all_gather(soft_k, SP, axis=1, tiled=True)]
    reduce_scatter x1, waiting for transfers between devices: 152 us -> 198 us  [shards(): lax.psum_scatter(term(jnp.int32(0), rows_dev * lax.axis_size(('fs', 'tp')...]
    all_to_all x0 -> x1, waiting for transfers between devices: none -> 39.2 us  [mixers(): lax.all_to_all(jnp.stack([soft_k] * lax.axis_size(SP)), SP, 0, 0)]
    all_to_all x0 -> x1, local copies, waits for them, and re-layouts: none -> 7.72 us  [mixers(): lax.all_to_all(jnp.stack([soft_k] * lax.axis_size(SP)), SP, 0, 0)]
    all_to_all x0 -> x1, starting transfers between devices: none -> 6.32 us  [mixers(): lax.all_to_all(jnp.stack([soft_k] * lax.axis_size(SP)), SP, 0, 0)]
  transfers between devices with their start and end apart: 7 -> 7, of which waited for: 6 -> 5; matrix products, arithmetic and copies ran while one was open for 11% -> 12% of each run, Pallas kernels for 0% -> 0%
where the time goes in v1:
time: 565 us; the launch traced here: 562 us
  waiting for transfers between devices  306 us (54%)
  blocking collectives  113 us (20%)
  matrix products  53 us (9%)
  local copies, waits for them, and re-layouts  37.1 us (7%)
  other arithmetic  31.8 us (6%)
  between operations  14.7 us (3%)
  starting transfers between devices  6.74 us (1%)
    reduce_scatter x1, waiting for transfers between devices, shards(): lax.psum_scatter(term(jnp.int32(0), rows_dev * lax.axis_size(('fs', 'tp')...  198 us
    all_gather x2, blocking collectives, carried_in(): lax.all_gather(part.astype(kind), axis)  103 us
    all_to_all x1, waiting for transfers between devices, mixers(): lax.all_to_all(jnp.stack([soft_k] * lax.axis_size(SP)), SP, 0, 0)  39.2 us
    all_gather x1, waiting for transfers between devices, shards(): lax.all_gather(normed, 'fs', axis=0, tiled=True)  39.1 us
    dot_general x7, matrix products, project(): product = jnp.dot(flat_rows, weight, preferred_element_type=jnp.float32)  19.5 us
    all_gather x1, waiting for transfers between devices, shards(): whole = lax.all_gather(tokens, 'tp', axis=2, tiled=True).astype(jnp.float32)  15.9 us
    reduce_sum x4, other arithmetic, advance(): jnp.sum(query_blk[:, :, :, None, :] * key_blk[:, :, None, :, :] * decay_p...  14.9 us
    all_gather x2, waiting for transfers between devices, carried_in(): lax.all_gather(part.astype(kind), axis)  13.3 us
  transfers between devices with their start and end apart: 7, of which 5 were waited for; matrix products, arithmetic and copies ran while one was open for 12% of the time, Pallas kernels for 0%

profile of v1, /device:TPU:0, one launch (start us, length us, event | category | flops | bytes accessed | tf_op | source)
XLA Modules:
  0.0 562.1 jit_solution(13624261122700873347)
XLA Ops:
  8.0 15.9 %all-gather.9.cloned.1.call-done = bf16[1,256,2048]{2,1,0:T(8,128)(2,1)} async-done(((bf16[1,256,1024]{2,1,0:T(8,128)(2,1)}), bf16[1,256,2048]{2,1,0:T(8,128)(2,1)}) %all-gather.9.cloned.1.call-update) | async-done | bytes 1048592 | tf_op jit(solution)/shard_map/all_gather | solution.py:307
  25.4 2.6 fusion.48
  28.1 9.8 %all_gather.34 = bf16[2,4,256]{2,0,1:T(2,128)(2,1)S(1)} all-gather(bf16[2,1,256]{2,0,1:T(2,128)(2,1)S(1)} %copy-done.14), channel_id=1, replica_groups=mesh['sp_0'=4,'sp_1'=4,'fs'=4,'tp'=2] {'fs'}, dimensions={1}, use_global_device_ids=true | all-gather | bytes 5120 | tf_op jit(solution)/shard_map/all_gather | solution.py:313
  38.6 39.1 %all-gather.11.cloned.1.call-done = bf16[4,256,2048]{2,1,0:T(8,128)(2,1)} async-done(((bf16[1,256,2048]{2,1,0:T(8,128)(2,1)}), bf16[4,256,2048]{2,1,0:T(8,128)(2,1)}) %all-gather.11.cloned.1.call-update) | async-done | bytes 4194320 | tf_op jit(solution)/shard_map/all_gather | solution.py:312
  77.7 3.8 fusion.102
  85.5 21.9 %while.44 = (s32[]{:T(128)}, f32[4,1,128,256]{3,2,0,1:T(8,128)S(1)}, f32[4,1,128]{2,0,1:T(4,128)S(1)}, f32[4,4,1,64,256]{4,3,0,1,2:T(8,128)}, bf16[4,4,1,64,128]...) while((s32[]{:T(128)}, ...), condition=%wide.region_4.5_spmd.clone, body=%wide.region_1.4_spmd.clone.sunk | while | flops 55235584 | bytes 4980881 | solution.py:107
  85.8 3.7 multiply_reduce_fusion.3
  91.3 3.7 multiply_reduce_fusion.3
  96.7 3.7 multiply_reduce_fusion.3
  102.2 3.7 multiply_reduce_fusion.3
  108.3 11.1 %all-gather = bf16[16,1,128]{2,1,0:T(2,128)(2,1)S(1)} all-gather(bf16[4,1,128]{2,1,0:T(2,128)(2,1)S(1)} %copy.151), channel_id=2, replica_groups=mesh['sp_0'=4,'sp_1'=4,'fs'=4,'tp'=2] {'sp_1'}, dimensions={0}, use_global_device_ids=true | all-gather | bytes 5120 | tf_op jit(solution)/shard_map/all_gather | solution.py:30
  119.5 13.3 %all-gather.15.cloned.1.call-done = bf16[16,1,128,256]{3,2,1,0:T(8,128)(2,1)} async-done(((bf16[4,1,128,256]{3,2,1,0:T(8,128)(2,1)}), bf16[16,1,128,256]{3,2,1,0:T(8,128)(2,1)}) %all-gather.15.cloned.1.call-update) | async-done | bytes 1048592 | tf_op jit(solution)/shard_map/all_gather | solution.py:30
  132.8 2.2 fusion.155
  135.9 3.8 convolution_convert_fusion.2
  140.4 4.6 convolution_convert_fusion
  145.1 3.6 convolution_convert_fusion.1
  151.1 2.4 copy.195
  153.5 2.7 subtract_convert_fusion
  156.5 5.3 stack.2
  161.9 6.3 %all-to-all-start = ((bf16[16,4,256,1,2,128]{5,2,4,1,3,0:T(8,128)(2,1)}), bf16[16,4,256,1,2,128]{5,2,4,1,3,0:T(8,128)(2,1)}, u32[]{:S(2)}, u32[]{:S(2)}) async-start(bf16[16,4,256,1,2,128]{5,2,4,1,3,0:T(8,128)(2,1)} %stack.2), calls=%async_computation | async-start | bytes 16777216 | tf_op jit(solution)/shard_map/all_to_all | solution.py:253
  169.0 91.7 %all_gather.37 = bf16[4,4,1,128]{3,1,2,0:T(4,128)(2,1)S(1)} all-gather(bf16[1,4,1,128]{3,1,2,0:T(4,128)(2,1)S(1)} %fusion.176), channel_id=1, replica_groups=mesh['sp_0'=4,'sp_1'=4,'fs'=4,'tp'=2] {'sp_0'}, dimensions={0}, use_global_device_ids=true | all-gather | bytes 5120 | tf_op jit(solution)/shard_map/all_gather | solution.py:30
  261.1 3.6 fusion.73
  276.5 39.2 %all-to-all-done = bf16[16,4,256,1,2,128]{5,2,4,1,3,0:T(8,128)(2,1)} async-done(((bf16[16,4,256,1,2,128]{5,2,4,1,3,0:T(8,128)(2,1)}), bf16[16,4,256,1,2,128]{5,2,4,1,3,0:T(8,128)(2,1)}, u32[]{:S(2)}, u32[]{:S(2)}) %all-to-all-start) | async-done | bytes 8388640 | tf_op jit(solution)/shard_map/all_to_all | solution.py:253
  315.8 7.7 %copy.170 = bf16[16,4,256,1,2,128]{5,2,0,4,1,3:T(8,128)(2,1)} copy(bf16[16,4,256,1,2,128]{5,2,4,1,3,0:T(8,128)(2,1)} %all-to-all-done) | data formatting | bytes 16777216 | tf_op jit(solution)/shard_map/all_to_all | solution.py:253
  323.5 11.1 %broadcast_in_dim.60 = f32[16,4,1,2,256,256]{4,5,3,1,2,0:T(8,128)} broadcast(f32[]{:T(128)} %constant.670.clone.1), dimensions={} | broadcast | bytes 33554436 | tf_op jit(solution)/shard_map/broadcast_in_dim | solution.py:146
  334.6 3.6 while.43
  339.0 7.7 %while.42 = (s32[]{:T(128)}, f32[4,1,256,256]{3,2,0,1:T(8,128)S(1)}, s32[]{:T(128)}, f32[16,4,1,2,256,256]{4,5,3,1,2,0:T(8,128)}, f32[4,1,2,256]{3,0,2,1:T(4,128...) while((s32[]{:T(128)}, ...), condition=%wide.region_11.12_spmd, body=%wide.region_10.11_spmd.sunk | while | flops 136314880 | bytes 17318612 | solution.py:170
  340.8 1.9 copy.225
  342.7 1.9 fusion.215
  344.6 2.0 fusion.216
  347.2 2.7 fusion.51
  357.7 197.6 %reduce-scatter.2.cloned.1.call-done = bf16[256,1024]{1,0:T(8,128)(2,1)} async-done(((bf16[2048,1024]{1,0:T(8,128)(2,1)}), bf16[256,1024]{1,0:T(8,128)(2,1)}) %reduce-scatter.2.cloned.1.call-update) | async-done | bytes 524304 | tf_op jit(solution)/shard_map/reduce_scatter | solution.py:343
  (177 shorter events, 46.1 us)
Async XLA Ops:
  7.2 74.3 %copy-start = (bf16[2048,256]{1,0:T(8,128)(2,1)S(1)}, bf16[2048,256]{1,0:T(8,128)(2,1)}, u32[]{:S(2)}) copy-start(bf16[2048,256]{1,0:T(8,128)(2,1)} %param.26) | copy-start | bytes 3145732
  7.2 20.9 %copy-start.14 = (bf16[2,1,256]{2,0,1:T(2,128)(2,1)S(1)}, bf16[2,1,256]{2,0,1:T(2,128)(2,1)}, u32[]{:S(2)}) copy-start(bf16[2,1,256]{2,0,1:T(2,128)(2,1)} %param.29) | copy-start | bytes 3076
  7.2 70.5 %copy-start.20 = (bf16[2048,128]{1,0:T(8,128)(2,1)S(1)}, bf16[2048,128]{1,0:T(8,128)(2,1)}, u32[]{:S(2)}) copy-start(bf16[2048,128]{1,0:T(8,128)(2,1)} %param.27) | copy-start | bytes 1572868
  7.2 16.7 %all-gather.9.cloned.1.call-start = ((), (), s32[]{:S(2)}) async-start(), calls=%async_computation.2 | async-start | bytes 1572864 | tf_op jit(solution)/shard_map/all_gather | solution.py:307
  7.9 69.7 %all-gather.11.cloned.1.call-start = ((), (), s32[]{:S(2)}) async-start(), calls=%async_computation.3 | async-start | bytes 5242880 | tf_op jit(solution)/shard_map/all_gather | solution.py:312
  28.0 104.8 %all-gather.15.cloned.1.call-start = ((), (), s32[]{:S(2)}) async-start(), calls=%async_computation.6 | async-start | bytes 1310720 | tf_op jit(solution)/shard_map/all_gather | solution.py:30
  77.7 3.8 copy-start.18
  81.5 1.3 copy-start.21
  82.8 1.3 copy-start.22
  107.4 0.9 copy-start.23
  108.2 152.9 %all-gather.13.cloned.1.call-start = ((), (), s32[]{:S(2)}) async-start(), calls=%async_computation.4 | async-start | bytes 1310720 | tf_op jit(solution)/shard_map/all_gather | solution.py:30
  135.1 203.8 %all-gather.17.cloned.1.call-start = ((), (), s32[]{:S(2)}) async-start(), calls=%async_computation.7 | async-start | bytes 8912896 | tf_op jit(solution)/shard_map/all_gather | solution.py:254
  140.4 4.7 copy-start.19
  161.9 6.4 %copy-start.17 = (f32[8]{0:T(128)S(1)}, f32[8]{0:T(128)}, u32[]{:S(2)}) copy-start(f32[8]{0:T(128)} %param.33) | copy-start | bytes 100
  161.9 98.9 %copy-start.11 = (bf16[4,256,1,2,64]{4,1,3,0,2:T(8,128)(2,1)S(1)}, bf16[4,256,1,2,64]{4,1,3,0,2:T(8,128)(2,1)}, u32[]{:S(2)}) copy-start(bf16[4,256,1,2,64]{4,1,3,0,2:T(8,128)(2,1)} %get-tuple-element.311) | copy-start | bytes 786436
  161.9 98.9 %copy-start.12 = (bf16[4,256,1,2,64]{4,1,3,0,2:T(8,128)(2,1)S(1)}, bf16[4,256,1,2,64]{4,1,3,0,2:T(8,128)(2,1)}, u32[]{:S(2)}) copy-start(bf16[4,256,1,2,64]{4,1,3,0,2:T(8,128)(2,1)} %get-tuple-element.312) | copy-start | bytes 786436
  161.9 99.2 %copy-start.13 = (bf16[16,1,128,256]{3,2,1,0:T(8,128)(2,1)S(1)}, bf16[16,1,128,256]{3,2,1,0:T(8,128)(2,1)}, u32[]{:S(2)}) copy-start(bf16[16,1,128,256]{3,2,1,0:T(8,128)(2,1)} %all-gather.15.cloned.1.call-done) | copy-start | bytes 3145732
  161.9 153.9 %all-to-all-start = ((bf16[16,4,256,1,2,128]{5,2,4,1,3,0:T(8,128)(2,1)}), bf16[16,4,256,1,2,128]{5,2,4,1,3,0:T(8,128)(2,1)}, u32[]{:S(2)}, u32[]{:S(2)}) async-start(bf16[16,4,256,1,2,128]{5,2,4,1,3,0:T(8,128)(2,1)} %stack.2), calls=%async_computation | async-start | bytes 16777216 | tf_op jit(solution)/shard_map/all_to_all | solution.py:253
  168.2 96.6 %copy-start.15 = (f32[256]{0:T(256)S(1)}, f32[256]{0:T(256)}, u32[]{:S(2)}) copy-start(f32[256]{0:T(256)} %param.34) | copy-start | bytes 3076
  168.2 387.1 %reduce-scatter.2.cloned.1.call-start = ((), (), s32[]{:S(2)}) async-start(), calls=%async_computation.5 | async-start | bytes 4718592 | tf_op jit(solution)/shard_map/reduce_scatter | solution.py:343
  261.0 5.2 copy-start.3
  338.9 8.0 %copy-start.16 = (f32[256]{0:T(256)S(1)}, f32[256]{0:T(256)}, u32[]{:S(2)}) copy-start(f32[256]{0:T(256)} %param.35) | copy-start | bytes 3076
  346.7 3.2 copy-start.2
  346.7 3.2 copy-start.10
  346.7 4.3 copy-start.9
  346.9 5.2 copy-start.8
  347.2 6.1 %copy-start.7 = (f32[256,1024]{1,0:T(8,128)S(1)}, f32[256,1024]{1,0:T(8,128)}, u32[]{:S(2)}) copy-start(f32[256,1024]{1,0:T(8,128)} %fusion.139) | copy-start | bytes 3145732
  349.9 4.5 copy-start.6
  351.0 4.4 copy-start.5
  352.1 4.4 copy-start.4
  354.4 200.9 %copy-start.1 = (bf16[2048,256]{1,0:T(8,128)(2,1)S(1)}, bf16[2048,256]{1,0:T(8,128)(2,1)}, u32[]{:S(2)}) copy-start(bf16[2048,256]{1,0:T(8,128)(2,1)} %param.26) | copy-start | bytes 3145732
Sparse Core Ops, SparseCore 0:
  9.7 14.1 all-gather.8
  28.1 49.5 all-gather.10
  108.3 24.4 all-gather.14
  135.2 24.6 all-gather.12
  161.9 163.6 all-gather.16
  357.8 197.4 reduce-scatter.1
